TPU v7x, 32 devices: a whole 2x2x4 slice. The times are simulated.
32 devices in a mesh: ep: 8 (over z, x), tp: 4 (over y, core).
Axes of the slice: x: 2, y: 2, z: 4, core: 2. Of those that a mesh axis runs over, the one named last changes fastest.
Arguments:
- mix_query: bfloat16 [2048, 2048], P('ep', 'tp'), may hold values from -6 to 6
- forget_input: bfloat16 [2048, 2048], P('ep', 'tp'), may hold values from -6 to 6
- mix_value: bfloat16 [2048, 2048], P('ep', 'tp'), may hold values from -6 to 6
- out_gate_input: bfloat16 [2048, 2048], P('ep', 'tp'), may hold values from -6 to 6
- decay_shift: float32 [2048, 16], P('ep', 'tp'), may hold values from -1.5 to 0
- forget_floor: float32 [2048], P('tp'), may hold values from 0.9 to 1
- head_gain: float32 [128], replicated, may hold values from 0.1 to 1.9
- w_mix_out: bfloat16 [2048, 2048], P(None, 'tp'), may hold values from -0.125 to 0.125
- moe_input: bfloat16 [2048, 2048], P('ep'), may hold values from -6 to 6
- moe_gain: float32 [2048], replicated, may hold values from 0.1 to 1.9
- routes: int32 [2048, 2], P('ep'), may hold values from 0 to 7, all different within a row; in each aligned block of 256 rows (0 to 255, 256 to 511, ...) at most 80 rows name the same one
- route_weight: float32 [2048, 2], P('ep'), may hold values from 0.1 to 1
- w_exp_gate: bfloat16 [8, 2048, 4096], P('ep', None, 'tp'), may hold values from -0.125 to 0.125
- w_exp_up: bfloat16 [8, 2048, 4096], P('ep', None, 'tp'), may hold values from -0.125 to 0.125
- w_exp_down: bfloat16 [8, 4096, 2048], P('ep', 'tp'), may hold values from -0.125 to 0.125
Outputs:
- mixed: bfloat16 [2048, 2048], P('ep', 'tp')
- moe_out: bfloat16 [2048, 2048], P('ep', 'tp')
Inputs may be any that keep to these rules, and one draw needn't show every extreme that they name: `routes`: at most 80 of the rows of one index of ep name one expert, and in every draw some device's rows name one expert exactly 80 times; the experts of a row differ.
All inputs are finite; a program needn't handle non-finite values.
Results may differ from a plain program's by a relative error of at most 0.02.
Values may be sent and summed in bfloat16 or wider, within the bound.
A program may use at most 64 MiB of HBM per device.

v0:
```python
import jax
import jax.numpy as jnp
from jax import lax
from jax.sharding import PartitionSpec as P

TOP_K = 2
eps = 1e-06
highest_precision = lax.Precision.HIGHEST


def carried_in(shard, axis, join, neutral):
    place = lax.axis_index(axis)
    gathered = jax.tree.map(
        lambda a, kind: lax.all_gather(a.astype(kind), axis), shard, (jnp.bfloat16, jnp.bfloat16)
    )
    state = jax.tree.map(lambda a, e: jnp.zeros_like(a) + jnp.asarray(e, a.dtype), shard, neutral)

    def one(turn, state):
        return join(
            state,
            jax.tree.map(
                lambda a, own: lax.dynamic_index_in_dim(a, turn, 0, False).astype(own.dtype),
                gathered,
                shard,
            ),
        )

    return lax.fori_loop(0, place, one, state)


def chain_step(earlier, later):
    return (earlier[0] * later[0], later[0][:, :, None] * earlier[1] + later[1])


def token_mixer(
    mix_query,
    forget_input,
    mix_value,
    out_gate_input,
    decay_shift,
    forget_floor,
    head_gain,
    w_mix_out,
):
    length = mix_query.shape[0]
    heads_here = decay_shift.shape[1]
    head_size = head_gain.shape[0]
    gate_input = forget_input.astype(jnp.float32)
    forget = forget_floor + (1.0 - forget_floor) * jax.nn.sigmoid(gate_input)
    input_gate = (1.0 - forget_floor) * jax.nn.sigmoid(-gate_input)
    log_decay = jnp.log(forget) + jnp.repeat(decay_shift, head_size, axis=1)

    def by_head(array):
        return array.reshape(length, heads_here, head_size).transpose(1, 0, 2)

    running_decay = jnp.cumsum(by_head(log_decay), axis=1)
    query_rows = by_head(mix_query.astype(jnp.float32)) * jnp.exp(running_decay)
    head_keys = by_head(input_gate)
    values = by_head(mix_value.astype(jnp.float32))
    scores = jnp.einsum(
        "htk,hsk->hts", query_rows, head_keys * jnp.exp(-running_decay), precision=highest_precision
    )
    causal = jnp.arange(length)[:, None] >= jnp.arange(length)[None, :]
    scores = jnp.where(causal[None, :, :], scores, 0.0)
    within_block_output = jnp.einsum("hts,hsv->htv", scores, values, precision=highest_precision)
    closing_total = running_decay[:, -1, :]
    carried_over_state = jnp.einsum(
        "gbx,gbi->gxi",
        head_keys * jnp.exp(closing_total[:, None, :] - running_decay),
        values,
        precision=highest_precision,
    )
    incoming_state = carried_in(
        (jnp.exp(closing_total), carried_over_state),
        "ep",
        chain_step,
        (jnp.ones_like(closing_total), jnp.zeros_like(carried_over_state)),
    )[1]
    block_result = within_block_output + jnp.einsum(
        "rsd,rda->rsa", query_rows, incoming_state, precision=highest_precision
    )
    inverse = lax.rsqrt(jnp.mean(block_result * block_result, axis=2, keepdims=True) + eps)
    gated = by_head(jax.nn.silu(out_gate_input.astype(jnp.float32)))
    normed_heads = (block_result * inverse * head_gain * gated).transpose(1, 0, 2)
    head_out = normed_heads.reshape(length, heads_here * head_size).astype(jnp.bfloat16)
    mixed = jnp.dot(
        lax.all_gather(head_out, "tp", axis=1, tiled=True),
        w_mix_out,
        preferred_element_type=jnp.float32,
    )
    return mixed.astype(jnp.bfloat16)


def experts_layer(moe_input, moe_gain, routes, route_weight, w_exp_gate, w_exp_up, w_exp_down):
    row_count = moe_input.shape[0]
    expert_count = lax.axis_size("ep")
    capacity = 5 * row_count * TOP_K // (4 * expert_count)
    token_rows = moe_input.astype(jnp.float32)
    inverse = lax.rsqrt(jnp.mean(token_rows * token_rows, axis=1, keepdims=True) + eps)
    normed = (token_rows * inverse * moe_gain).astype(jnp.bfloat16)
    flat_ids = routes.reshape(-1)
    pair_count = flat_ids.shape[0]
    one_hot = (flat_ids[:, None] == jnp.arange(expert_count, dtype=jnp.int32)[None, :]).astype(
        jnp.int32
    )
    earlier_count = jnp.cumsum(one_hot, axis=0) - one_hot
    ranks = jnp.sum(earlier_count * one_hot, axis=1)
    slot_ids = flat_ids * capacity + ranks
    owners = (
        jnp.zeros((expert_count * capacity,), jnp.int32)
        .at[slot_ids]
        .set(jnp.arange(pair_count, dtype=jnp.int32) // TOP_K)
    )
    filled = (
        jnp.zeros((expert_count * capacity,), jnp.bfloat16)
        .at[slot_ids]
        .set(jnp.ones((pair_count,), jnp.bfloat16))
    )
    outgoing = normed[owners] * filled[:, None]
    w_gate = w_exp_gate[0]
    w_up = w_exp_up[0]
    w_down = w_exp_down[0]
    width = normed.shape[1] // lax.axis_size("tp")
    own_slice = lax.dynamic_slice_in_dim(outgoing, lax.axis_index("tp") * width, width, 1)
    arrived = lax.all_to_all(own_slice, "ep", split_axis=0, concat_axis=0, tiled=True)
    portion = lax.all_gather(arrived, "tp", axis=1, tiled=True)
    gate_sum = jnp.dot(portion, w_gate, preferred_element_type=jnp.float32)
    up_sum = jnp.dot(portion, w_up, preferred_element_type=jnp.float32)
    hidden = (jax.nn.silu(gate_sum) * up_sum).astype(jnp.bfloat16)
    partial_value = jnp.dot(hidden, w_down, preferred_element_type=jnp.float32)
    summed = lax.psum_scatter(
        partial_value.astype(jnp.bfloat16), "tp", scatter_dimension=1, tiled=True
    )
    returned = lax.all_to_all(summed, "ep", split_axis=0, concat_axis=0, tiled=True)
    picked = returned[slot_ids].astype(jnp.float32).reshape(row_count, TOP_K, returned.shape[1])
    combined = jnp.sum(picked * route_weight[:, :, None], axis=1)
    return combined.astype(jnp.bfloat16)


def body(
    mix_query,
    forget_input,
    mix_value,
    out_gate_input,
    decay_shift,
    forget_floor,
    head_gain,
    w_mix_out,
    moe_input,
    moe_gain,
    routes,
    route_weight,
    w_exp_gate,
    w_exp_up,
    w_exp_down,
):
    mixed = token_mixer(
        mix_query,
        forget_input,
        mix_value,
        out_gate_input,
        decay_shift,
        forget_floor,
        head_gain,
        w_mix_out,
    )
    moe_out = experts_layer(
        moe_input, moe_gain, routes, route_weight, w_exp_gate, w_exp_up, w_exp_down
    )
    return (mixed, moe_out)


def solution(mesh):
    placed = (
        P("ep", "tp"),
        P("ep", "tp"),
        P("ep", "tp"),
        P("ep", "tp"),
        P("ep", "tp"),
        P("tp"),
        P(),
        P(None, "tp"),
        P("ep", None),
        P(),
        P("ep", None),
        P("ep", None),
        P("ep", None, "tp"),
        P("ep", None, "tp"),
        P("ep", "tp", None),
    )
    return jax.shard_map(
        body, mesh=mesh, in_specs=placed, out_specs=(P("ep", "tp"), P("ep", "tp")), check_vma=False
    )
```

profile of v0, /device:TPU:0, one launch (start us, length us, event | category | flops | bytes accessed | tf_op | source)
XLA Modules:
  0.0 189.2 jit_solution(8927491651452208620)
XLA Ops:
  7.2 0.9 copy.108
  8.2 0.1 eq.29
  8.3 0.1 eq.25
  8.5 0.7 broadcast_multiply_fusion
  9.2 1.1 reduce-window.16
  10.3 0.2 slice_reduce_fusion
  10.6 0.1 copy.107
  10.7 0.1 mul.149
  10.9 0.1 fusion.42
  11.0 2.4 %scatter_custom_fusion = s32[640]{0:T(1024)S(1)} fusion(s32[512]{0:T(512)S(1)} %bitcast.123, s32[512]{0:T(512)S(1)} %add_select_fusion, s32[]{:T(128)} %constant.68.clone.1), kind=kCustom, calls=%fused_computation.82 | custom fusion | bytes 2564 | tf_op jit(solution)/shard_map/scatter | solution.py:112
  13.5 1.5 fusion.9
  15.0 1.5 fusion.11
  16.5 4.1 %gather_fusion = bf16[640,2048]{1,0:T(8,128)(2,1)} fusion(bf16[256,2048]{1,0:T(8,128)(2,1)S(1)} %fusion.11, s32[1024]{0:T(1024)S(1)} %pad_clamp_fusion.1), kind=kCustom, calls=%fused_computation | custom fusion | bytes 5245440 | tf_op jit(solution)/shard_map/gather | solution.py:119
  20.6 3.8 %scatter_custom_fusion.1 = bf16[640]{0:T(1024)(128)(2,1)S(1)} fusion(s32[512]{0:T(512)S(1)} %bitcast.124, bf16[512]{0:T(512)(128)(2,1)S(1)} %broadcast.119, bf16[]{:T(256)} %constant.79.clone.1), kind=kCustom, calls=%fused_computation.87 | custom fusion | bytes 1282 | tf_op jit(solution)/shard_map/scatter | solution.py:117
  24.4 1.3 dynamic-slice_multiply_fusion
  25.7 24.9 %all_to_all.24 = bf16[8,80,512]{2,1,0:T(8,128)(2,1)} all-to-all(bf16[8,80,512]{2,1,0:T(8,128)(2,1)S(1)} %bitcast.112), channel_id=1, replica_groups=mesh['ep'=8,'tp'=4] {'ep'}, dimensions={0} | all-to-all | bytes 1310720 | tf_op jit(solution)/shard_map/all_to_all | solution.py:125
  50.6 0.1 copy.92
  50.8 1.1 fusion.25
  51.9 0.2 copy.93
  52.1 0.4 fusion.34
  52.5 0.2 broadcast_add_fusion
  52.8 1.1 copy.144
  53.9 2.2 %copy.97 = f32[256,4,128]{2,1,0:T(4,128)} copy(f32[256,4,128]{0,2,1:T(8,128)} %bitcast.114) | data formatting | bytes 1048576 | tf_op jit(solution)/shard_map/reshape | solution.py:54
  56.1 1.1 copy.90
  57.2 0.9 copy.91
  58.1 0.7 slice_bitcast_fusion.1
  58.8 2.8 %bitcast_multiply_fusion.2 = (f32[4,256,128]{2,0,1:T(4,128)}, f32[4,256,128]{2,0,1:T(4,128)S(1)}, f32[4,256,128]{2,0,1:T(4,128)S(1)}) fusion(f32[256,4,128]{2,1,0:T(4,128)} %copy.97, f32[4,128,256]{1,2,0:T(8,128)S(1)} %bitcast.110, f32[4,128]{1,0:T(4,128)S(1)} %get-tuple-element.60, f32[256,4,128]{2,1,0:T(4,128)} %copy.91), kind=kLoop, calls=%fused_computation.47 | loop fusion | flops 655360 | bytes 3147776 | tf_op jit(solution)/shard_map/mul | solution.py:61
  61.5 1.3 convolution_convert_fusion.1
  62.9 0.2 reduce-scatter.2.cloned.1.call-start
  63.1 11.9 %all-gather.8.cloned.1.call-done = bf16[640,2048]{1,0:T(8,128)(2,1)} async-done(((bf16[640,512]{1,0:T(8,128)(2,1)}), bf16[640,2048]{1,0:T(8,128)(2,1)}) %all-gather.8.cloned.1.call-update) | async-done | bytes 2621456 | tf_op jit(solution)/shard_map/all_gather | solution.py:126
  75.0 7.4 %fusion.2 = f32[640,1024]{1,0:T(8,128)} fusion(bf16[640,2048]{1,0:T(8,128)(2,1)} %all-gather.8.cloned.1.call-done, bf16[1,2048,1024]{2,1,0:T(8,128)(2,1)} %param.30), kind=kOutput, calls=%fused_computation.8 | convolution fusion | flops 2684354560 | bytes 9437184 | tf_op jit(solution)/shard_map/dot_general | solution.py:128
  82.3 12.5 %fusion.6 = bf16[640,2048]{1,0:T(8,128)(2,1)} fusion(bf16[1,1024,2048]{2,1,0:T(8,128)(2,1)} %param.31, f32[640,1024]{1,0:T(8,128)} %fusion.2, bf16[640,2048]{1,0:T(8,128)(2,1)} %all-gather.8.cloned.1.call-done, bf16[1,2048,1024]{2,1,0:T(8,128)(2,1)} %param.29), kind=kOutput, calls=%fused_computation.12 | convolution fusion | flops 5373952000 | bytes 16252928 | tf_op jit(solution)/shard_map/dot_general | solution.py:130
  94.9 26.4 %all-gather = bf16[32,1,128]{2,1,0:T(2,128)(2,1)S(1)} all-gather(bf16[4,1,128]{2,1,0:T(2,128)(2,1)S(1)} %copy.102), channel_id=2, replica_groups=mesh['ep'=8,'tp'=4] {'ep'}, dimensions={0}, use_global_device_ids=true | all-gather | bytes 9216 | tf_op jit(solution)/shard_map/all_gather | solution.py:14
  121.3 0.1 copy.106
  121.5 0.1 convert_multiply_fusion.2
  121.6 3.0 %convolution_select_fusion = f32[4,256,256]{2,1,0:T(8,128)} fusion(f32[4,256,128]{2,0,1:T(4,128)} %get-tuple-element.57, pred[256,256]{1,0:T(8,128)(4,1)S(1)} %iota_compare_fusion, f32[4,256,128]{2,0,1:T(4,128)S(1)} %get-tuple-element.59), kind=kOutput, calls=%fused_computation.19 | convolution fusion | flops 402915328 | bytes 2162688 | tf_op jit(solution)/shard_map/htk,hsk->hts/dot_general | solution.py:60
  124.7 0.6 fusion.36
  125.4 2.2 %multiply_reduce_fusion.1 = (f32[4,256]{1,0:T(4,128)S(1)}, f32[4,256,128]{1,2,0:T(8,128)S(1)}) fusion(f32[4,256,128]{1,2,0:T(8,128)S(1)} %fusion.36, f32[4,256,256]{2,1,0:T(8,128)} %convolution_select_fusion, bf16[256,512]{1,0:T(8,128)(2,1)} %param.19), kind=kOutput, calls=%fused_computation.54 | convolution fusion | flops 403045376 | bytes 2363392 | tf_op jit(solution)/shard_map/hts,hsv->htv/dot_general | solution.py:65
  127.6 0.8 fusion.31
  128.4 25.2 %reduce-scatter.2.cloned.1.call-done = bf16[640,512]{1,0:T(8,128)(2,1)} async-done(((bf16[640,2048]{1,0:T(8,128)(2,1)}), bf16[640,512]{1,0:T(8,128)(2,1)}) %reduce-scatter.2.cloned.1.call-update) | async-done | bytes 655376 | tf_op jit(solution)/shard_map/reduce_scatter | solution.py:131
  153.7 5.5 %all-to-all-start.1 = ((bf16[8,80,512]{2,1,0:T(8,128)(2,1)}), bf16[8,80,512]{2,1,0:T(8,128)(2,1)S(1)}, u32[]{:S(2)}, u32[]{:S(2)}) async-start(bf16[8,80,512]{2,1,0:T(8,128)(2,1)} %bitcast.119), calls=%async_computation.2 | async-start | bytes 1310720 | tf_op jit(solution)/shard_map/all_to_all | solution.py:134
  159.2 0.1 copy.110
  159.3 13.1 %all-gather.6.cloned.1.call-done = bf16[256,2048]{0,1:T(8,128)(2,1)} async-done(((bf16[256,512]{0,1:T(8,128)(2,1)}), bf16[256,2048]{0,1:T(8,128)(2,1)}) %all-gather.6.cloned.1.call-update) | async-done | bytes 1048592 | tf_op jit(solution)/shard_map/all_gather | solution.py:87
  172.4 2.7 %convolution_convert_fusion = bf16[256,512]{1,0:T(8,128)(2,1)} fusion(bf16[256,2048]{0,1:T(8,128)(2,1)} %all-gather.6.cloned.1.call-done, bf16[2048,512]{1,0:T(8,128)(2,1)S(1)} %copy-done), kind=kOutput, calls=%fused_computation.21 | convolution fusion | flops 537001984 | bytes 3407872 | tf_op jit(solution)/shard_map/dot_general | solution.py:86
  175.0 1.3 all-to-all-done.1
  176.3 2.6 %gather_fusion.1 = bf16[512,512]{1,0:T(8,128)(2,1)} fusion(bf16[640,512]{1,0:T(8,128)(2,1)S(1)} %bitcast.108, s32[1024]{0:T(1024)S(1)} %pad_clamp_fusion), kind=kCustom, calls=%fused_computation.1 | custom fusion | bytes 1050624 | tf_op jit(solution)/shard_map/gather | solution.py:135
  178.9 1.7 reshape.158
  180.6 2.1 %multiply_reduce_fusion = bf16[256,512]{1,0:T(8,128)(2,1)} fusion(f32[256,2,512]{2,1,0:T(2,128)S(1)} %reshape.158, f32[256,2]{1,0:T(8,128)S(1)} %copy.110), kind=kLoop, calls=%fused_computation.23 | loop fusion | flops 393216 | bytes 1312768 | tf_op jit(solution)/shard_map/reduce_sum | solution.py:136
  (45 shorter events, 0.5 us)
Async XLA Ops:
  7.2 165.2 %copy-start = (bf16[2048,512]{1,0:T(8,128)(2,1)S(1)}, bf16[2048,512]{1,0:T(8,128)(2,1)}, u32[]{:S(2)}) copy-start(bf16[2048,512]{1,0:T(8,128)(2,1)} %param.24) | copy-start | bytes 6291460
  7.2 67.8 %all-gather.8.cloned.1.call-start = ((), (), s32[]{:S(2)}) async-start(), calls=%async_computation.4 | async-start | bytes 3276800 | tf_op jit(solution)/shard_map/all_gather | solution.py:126
  20.6 30.0 %copy-start.2 = (bf16[256,512]{1,0:T(8,128)(2,1)S(1)}, bf16[256,512]{1,0:T(8,128)(2,1)}, u32[]{:S(2)}) copy-start(bf16[256,512]{1,0:T(8,128)(2,1)} %param.18) | copy-start | bytes 786436
  20.6 30.2 %copy-start.4 = (f32[512]{0:T(512)S(1)}, f32[512]{0:T(512)}, u32[]{:S(2)}) copy-start(f32[512]{0:T(512)} %param.22) | copy-start | bytes 6148
  20.6 30.2 %copy-start.5 = (f32[256,4]{0,1:T(4,128)S(1)}, f32[256,4]{0,1:T(4,128)}, u32[]{:S(2)}) copy-start(f32[256,4]{0,1:T(4,128)} %param.21) | copy-start | bytes 12292
  50.6 74.1 %all-gather.10.cloned.1.call-start = ((), (), s32[]{:S(2)}) async-start(), calls=%async_computation.6 | async-start | bytes 1179648 | tf_op jit(solution)/shard_map/all_gather | solution.py:14
  53.9 7.6 %copy-start.1 = (bf16[256,512]{1,0:T(8,128)(2,1)S(1)}, bf16[256,512]{1,0:T(8,128)(2,1)}, u32[]{:S(2)}) copy-start(bf16[256,512]{1,0:T(8,128)(2,1)} %param.19) | copy-start | bytes 786436
  62.9 90.8 %reduce-scatter.2.cloned.1.call-start = ((), (), s32[]{:S(2)}) async-start(), calls=%async_computation.5 | async-start | bytes 3276800 | tf_op jit(solution)/shard_map/reduce_scatter | solution.py:131
  94.8 26.5 %copy-start.3 = (bf16[256,512]{1,0:T(8,128)(2,1)S(1)}, bf16[256,512]{1,0:T(8,128)(2,1)}, u32[]{:S(2)}) copy-start(bf16[256,512]{1,0:T(8,128)(2,1)} %param.20) | copy-start | bytes 786436
  94.8 77.6 %all-gather.6.cloned.1.call-start = ((), (), s32[]{:S(2)}) async-start(), calls=%async_computation.3 | async-start | bytes 1310720 | tf_op jit(solution)/shard_map/all_gather | solution.py:87
  124.7 2.9 %copy-start.7 = (f32[128]{0:T(128)S(1)}, f32[128]{0:T(128)}, u32[]{:S(2)}) copy-start(f32[128]{0:T(128)} %param.23) | copy-start | bytes 1540
  125.4 33.8 %copy-start.6 = (f32[256,2]{0,1:T(2,128)S(1)}, f32[256,2]{0,1:T(2,128)}, u32[]{:S(2)}) copy-start(f32[256,2]{0,1:T(2,128)} %param.28) | copy-start | bytes 6148
  153.7 22.6 %all-to-all-start.1 = ((bf16[8,80,512]{2,1,0:T(8,128)(2,1)}), bf16[8,80,512]{2,1,0:T(8,128)(2,1)S(1)}, u32[]{:S(2)}, u32[]{:S(2)}) async-start(bf16[8,80,512]{2,1,0:T(8,128)(2,1)} %bitcast.119), calls=%async_computation.2 | async-start | bytes 1310720 | tf_op jit(solution)/shard_map/all_to_all | solution.py:134
Sparse Core Ops, SparseCore 0:
  50.7 24.2 all-gather.7
  77.7 40.3 all-gather.9
  120.5 33.0 reduce-scatter.1
  155.7 16.6 all-gather.5
where the time goes:
time: 190 us; the launch traced here: 189 us
  waiting for transfers between devices  51.5 us (27%)
  blocking collectives  51.3 us (27%)
  matrix products  29.7 us (16%)
  local copies, waits for them, and re-layouts  22.4 us (12%)
  other arithmetic  14.5 us (8%)
  between operations  14 us (7%)
  starting transfers between devices  5.83 us (3%)
    all_gather x1, blocking collectives, carried_in(): lax.all_gather(a.astype(kind), axis)  26.4 us
    reduce_scatter x1, waiting for transfers between devices, experts_layer(): lax.psum_scatter(partial_value.astype(jnp.bfloat16), 'tp', scatter_dimens...  25.2 us
    all_to_all x1, blocking collectives, experts_layer(): lax.all_to_all(own_slice, 'ep', split_axis=0, concat_axis=0, tiled=True)  24.9 us
    all_gather x1, waiting for transfers between devices, token_mixer(): lax.all_gather(head_out, 'tp', axis=1, tiled=True)  13.1 us
    dot_general x1, matrix products, experts_layer(): partial_value = jnp.dot(hidden, w_down, preferred_element_type=jnp.float32)  12.5 us
    all_gather x1, waiting for transfers between devices, experts_layer(): portion = lax.all_gather(arrived, 'tp', axis=1, tiled=True)  11.9 us
    dot_general x1, matrix products, experts_layer(): up_sum = jnp.dot(portion, w_up, preferred_element_type=jnp.float32)  7.36 us
    all_to_all x1, starting transfers between devices, experts_layer(): lax.all_to_all(summed, 'ep', split_axis=0, concat_axis=0, tiled=True)  5.49 us
  transfers between devices with their start and end apart: 5, of which 4 were waited for; matrix products, arithmetic and copies ran while one was open for 22% of the time, Pallas kernels for 0%

commit v1 on v0

--- a/solution.py
+++ b/solution.py
@@ -83,11 +83,11 @@
     gated = by_head(jax.nn.silu(out_gate_input.astype(jnp.float32)))
     normed_heads = (block_result * inverse * head_gain * gated).transpose(1, 0, 2)
     head_out = normed_heads.reshape(length, heads_here * head_size).astype(jnp.bfloat16)
-    mixed = jnp.dot(
-        lax.all_gather(head_out, "tp", axis=1, tiled=True),
-        w_mix_out,
-        preferred_element_type=jnp.float32,
-    )
+
+    def _check_members_all(packet):
+        return jnp.concatenate(jax.lax.all_gather(packet, axis_name="tp"), 1)
+
+    mixed = jnp.dot(_check_members_all(head_out), w_mix_out, preferred_element_type=jnp.float32)
     return mixed.astype(jnp.bfloat16)
 
 

time: 190 us -> 191 us (level)
  local copies, waits for them, and re-layouts: 22.4 us -> 25.5 us
    all_gather x0 -> x1, local copies, waits for them, and re-layouts: none -> 2.28 us  [_check_members_all(): return jnp.concatenate(jax.lax.all_gather(packet, axis_name='tp'), 1)]
  transfers between devices with their start and end apart: 5 -> 5, of which waited for: 4 -> 3; matrix products, arithmetic and copies ran while one was open for 22% -> 23% of each run, Pallas kernels for 0% -> 0%
where the time goes in v1:
time: 191 us; the launch traced here: 190 us
  blocking collectives  51.3 us (27%)
  waiting for transfers between devices  50.1 us (26%)
  matrix products  29.7 us (16%)
  local copies, waits for them, and re-layouts  25.5 us (13%)
  between operations  14.1 us (7%)
  other arithmetic  13.8 us (7%)
  starting transfers between devices  5.83 us (3%)
    all_gather x1, blocking collectives, carried_in(): lax.all_gather(a.astype(kind), axis)  26.4 us
    reduce_scatter x1, waiting for transfers between devices, experts_layer(): lax.psum_scatter(partial_value.astype(jnp.bfloat16), 'tp', scatter_dimens...  25.1 us
    all_to_all x1, blocking collectives, experts_layer(): lax.all_to_all(own_slice, 'ep', split_axis=0, concat_axis=0, tiled=True)  24.9 us
    all_gather x1, waiting for transfers between devices, _check_members_all(): return jnp.concatenate(jax.lax.all_gather(packet, axis_name='tp'), 1)  13.1 us
    dot_general x1, matrix products, experts_layer(): partial_value = jnp.dot(hidden, w_down, preferred_element_type=jnp.float32)  12.5 us
    all_gather x1, waiting for transfers between devices, experts_layer(): portion = lax.all_gather(arrived, 'tp', axis=1, tiled=True)  11.9 us
    dot_general x1, matrix products, experts_layer(): up_sum = jnp.dot(portion, w_up, preferred_element_type=jnp.float32)  7.36 us
    all_to_all x1, starting transfers between devices, experts_layer(): lax.all_to_all(summed, 'ep', split_axis=0, concat_axis=0, tiled=True)  5.49 us
  transfers between devices with their start and end apart: 5, of which 3 were waited for; matrix products, arithmetic and copies ran while one was open for 23% of the time, Pallas kernels for 0%

profile of v1, /device:TPU:0, one launch (start us, length us, event | category | flops | bytes accessed | tf_op | source)
XLA Modules:
  0.0 190.2 jit_solution(14634247104931802326)
XLA Ops:
  7.2 0.9 copy.131
  8.2 0.1 eq.29
  8.3 0.1 eq.25
  8.5 0.7 broadcast_multiply_fusion
  9.2 1.1 reduce-window.16
  10.3 0.2 slice_reduce_fusion
  10.6 0.1 copy.130
  10.7 0.1 mul.149
  11.0 2.4 %scatter_custom_fusion = s32[640]{0:T(1024)S(1)} fusion(s32[512]{0:T(512)S(1)} %bitcast.127, s32[512]{0:T(512)S(1)} %add_select_fusion, s32[]{:T(128)} %constant.68.clone.1), kind=kCustom, calls=%fused_computation.82 | custom fusion | bytes 2564 | tf_op jit(solution)/shard_map/scatter | solution.py:112
  13.5 1.5 fusion.9
  15.0 1.5 fusion.11
  16.5 4.1 %gather_fusion = bf16[640,2048]{1,0:T(8,128)(2,1)} fusion(bf16[256,2048]{1,0:T(8,128)(2,1)S(1)} %fusion.11, s32[1024]{0:T(1024)S(1)} %pad_clamp_fusion.1), kind=kCustom, calls=%fused_computation | custom fusion | bytes 5245440 | tf_op jit(solution)/shard_map/gather | solution.py:119
  20.6 3.8 %scatter_custom_fusion.1 = bf16[640]{0:T(1024)(128)(2,1)S(1)} fusion(s32[512]{0:T(512)S(1)} %bitcast.128, bf16[512]{0:T(512)(128)(2,1)S(1)} %broadcast.119, bf16[]{:T(256)} %constant.79.clone.1), kind=kCustom, calls=%fused_computation.87 | custom fusion | bytes 1282 | tf_op jit(solution)/shard_map/scatter | solution.py:117
  24.4 1.3 dynamic-slice_multiply_fusion
  25.7 24.9 %all_to_all.24 = bf16[8,80,512]{2,1,0:T(8,128)(2,1)} all-to-all(bf16[8,80,512]{2,1,0:T(8,128)(2,1)S(1)} %bitcast.115), channel_id=1, replica_groups=mesh['ep'=8,'tp'=4] {'ep'}, dimensions={0} | all-to-all | bytes 1310720 | tf_op jit(solution)/shard_map/all_to_all | solution.py:125
  50.6 0.1 copy.113
  50.8 1.1 fusion.25
  51.9 0.2 copy.114
  52.1 0.4 fusion.34
  52.5 0.2 broadcast_add_fusion
  52.8 1.1 copy.167
  53.9 2.2 %copy.118 = f32[256,4,128]{2,1,0:T(4,128)} copy(f32[256,4,128]{0,2,1:T(8,128)} %bitcast.117) | data formatting | bytes 1048576 | tf_op jit(solution)/shard_map/reshape | solution.py:54
  56.1 1.1 copy.111
  57.2 0.9 copy.112
  58.1 0.7 slice_bitcast_fusion.1
  58.8 2.8 %bitcast_multiply_fusion.2 = (f32[4,256,128]{2,0,1:T(4,128)}, f32[4,256,128]{2,0,1:T(4,128)S(1)}, f32[4,256,128]{2,0,1:T(4,128)S(1)}) fusion(f32[256,4,128]{2,1,0:T(4,128)} %copy.118, f32[4,128,256]{1,2,0:T(8,128)S(1)} %bitcast.113, f32[4,128]{1,0:T(4,128)S(1)} %get-tuple-element.60, f32[256,4,128]{2,1,0:T(4,128)} %copy.112), kind=kLoop, calls=%fused_computation.47 | loop fusion | flops 655360 | bytes 3147776 | tf_op jit(solution)/shard_map/mul | solution.py:61
  61.5 1.3 convolution_convert_fusion.1
  62.9 0.2 reduce-scatter.2.cloned.1.call-start
  63.1 11.9 %all-gather.8.cloned.1.call-done = bf16[640,2048]{1,0:T(8,128)(2,1)} async-done(((bf16[640,512]{1,0:T(8,128)(2,1)}), bf16[640,2048]{1,0:T(8,128)(2,1)}) %all-gather.8.cloned.1.call-update) | async-done | bytes 2621456 | tf_op jit(solution)/shard_map/all_gather | solution.py:126
  75.0 7.4 %fusion.2 = f32[640,1024]{1,0:T(8,128)} fusion(bf16[640,2048]{1,0:T(8,128)(2,1)} %all-gather.8.cloned.1.call-done, bf16[1,2048,1024]{2,1,0:T(8,128)(2,1)} %param.30), kind=kOutput, calls=%fused_computation.8 | convolution fusion | flops 2684354560 | bytes 9437184 | tf_op jit(solution)/shard_map/dot_general | solution.py:128
  82.3 12.5 %fusion.6 = bf16[640,2048]{1,0:T(8,128)(2,1)} fusion(bf16[1,1024,2048]{2,1,0:T(8,128)(2,1)} %param.31, f32[640,1024]{1,0:T(8,128)} %fusion.2, bf16[640,2048]{1,0:T(8,128)(2,1)} %all-gather.8.cloned.1.call-done, bf16[1,2048,1024]{2,1,0:T(8,128)(2,1)} %param.29), kind=kOutput, calls=%fused_computation.12 | convolution fusion | flops 5373952000 | bytes 16252928 | tf_op jit(solution)/shard_map/dot_general | solution.py:130
  94.9 26.4 %all-gather = bf16[32,1,128]{2,1,0:T(2,128)(2,1)S(1)} all-gather(bf16[4,1,128]{2,1,0:T(2,128)(2,1)S(1)} %copy.123), channel_id=2, replica_groups=mesh['ep'=8,'tp'=4] {'ep'}, dimensions={0}, use_global_device_ids=true | all-gather | bytes 9216 | tf_op jit(solution)/shard_map/all_gather | solution.py:14
  121.3 0.1 copy.127
  121.5 0.1 convert_multiply_fusion.2
  121.6 3.0 %convolution_select_fusion = f32[4,256,256]{2,1,0:T(8,128)} fusion(f32[4,256,128]{2,0,1:T(4,128)} %get-tuple-element.57, pred[256,256]{1,0:T(8,128)(4,1)S(1)} %iota_compare_fusion, f32[4,256,128]{2,0,1:T(4,128)S(1)} %get-tuple-element.59), kind=kOutput, calls=%fused_computation.19 | convolution fusion | flops 402915328 | bytes 2162688 | tf_op jit(solution)/shard_map/htk,hsk->hts/dot_general | solution.py:60
  124.7 0.6 fusion.36
  125.4 2.2 %multiply_reduce_fusion.1 = (f32[4,256]{1,0:T(4,128)S(1)}, f32[4,256,128]{1,2,0:T(8,128)S(1)}) fusion(f32[4,256,128]{1,2,0:T(8,128)S(1)} %fusion.36, f32[4,256,256]{2,1,0:T(8,128)} %convolution_select_fusion, bf16[256,512]{1,0:T(8,128)(2,1)} %param.19), kind=kOutput, calls=%fused_computation.54 | convolution fusion | flops 403045376 | bytes 2363392 | tf_op jit(solution)/shard_map/hts,hsv->htv/dot_general | solution.py:65
  127.6 0.1 fusion.31
  127.7 0.8 copy.128
  128.6 25.1 %reduce-scatter.2.cloned.1.call-done = bf16[640,512]{1,0:T(8,128)(2,1)} async-done(((bf16[640,2048]{1,0:T(8,128)(2,1)}), bf16[640,512]{1,0:T(8,128)(2,1)}) %reduce-scatter.2.cloned.1.call-update) | async-done | bytes 655376 | tf_op jit(solution)/shard_map/reduce_scatter | solution.py:131
  153.7 5.5 %all-to-all-start.1 = ((bf16[8,80,512]{2,1,0:T(8,128)(2,1)}), bf16[8,80,512]{2,1,0:T(8,128)(2,1)S(1)}, u32[]{:S(2)}, u32[]{:S(2)}) async-start(bf16[8,80,512]{2,1,0:T(8,128)(2,1)} %bitcast.123), calls=%async_computation.2 | async-start | bytes 1310720 | tf_op jit(solution)/shard_map/all_to_all | solution.py:134
  159.2 0.1 copy.133
  159.3 13.1 %all-gather.6.cloned.1.call-done = bf16[4,256,512]{2,1,0:T(8,128)(2,1)} async-done(((bf16[1,256,512]{2,1,0:T(8,128)(2,1)}), bf16[4,256,512]{2,1,0:T(8,128)(2,1)}) %all-gather.6.cloned.1.call-update) | async-done | bytes 1048592 | tf_op jit(solution)/shard_map/all_gather | solution.py:88
  172.4 2.3 %copy.129 = bf16[4,256,512]{1,2,0:T(8,128)(2,1)} copy(bf16[4,256,512]{2,1,0:T(8,128)(2,1)} %all-gather.6.cloned.1.call-done) | data formatting | bytes 2097152 | tf_op jit(solution)/shard_map/all_gather | solution.py:88
  174.7 2.7 %convolution_convert_fusion = bf16[256,512]{1,0:T(8,128)(2,1)} fusion(bf16[256,2048]{0,1:T(8,128)(2,1)} %bitcast.122, bf16[2048,512]{1,0:T(8,128)(2,1)S(1)} %copy-done), kind=kOutput, calls=%fused_computation.21 | convolution fusion | flops 537001984 | bytes 3407872 | tf_op jit(solution)/shard_map/dot_general | solution.py:90
  177.3 2.6 %gather_fusion.1 = bf16[512,512]{1,0:T(8,128)(2,1)} fusion(bf16[640,512]{1,0:T(8,128)(2,1)S(1)} %bitcast.111, s32[1024]{0:T(1024)S(1)} %pad_clamp_fusion), kind=kCustom, calls=%fused_computation.1 | custom fusion | bytes 1050624 | tf_op jit(solution)/shard_map/gather | solution.py:135
  179.9 1.7 reshape.176
  181.6 2.1 %multiply_reduce_fusion = bf16[256,512]{1,0:T(8,128)(2,1)} fusion(f32[256,2,512]{2,1,0:T(2,128)S(1)} %reshape.176, f32[256,2]{1,0:T(8,128)S(1)} %copy.133), kind=kLoop, calls=%fused_computation.23 | loop fusion | flops 393216 | bytes 1312768 | tf_op jit(solution)/shard_map/reduce_sum | solution.py:136
  (47 shorter events, 0.6 us)
Async XLA Ops:
  7.2 167.5 %copy-start = (bf16[2048,512]{1,0:T(8,128)(2,1)S(1)}, bf16[2048,512]{1,0:T(8,128)(2,1)}, u32[]{:S(2)}) copy-start(bf16[2048,512]{1,0:T(8,128)(2,1)} %param.24) | copy-start | bytes 6291460
  7.2 67.8 %all-gather.8.cloned.1.call-start = ((), (), s32[]{:S(2)}) async-start(), calls=%async_computation.4 | async-start | bytes 3276800 | tf_op jit(solution)/shard_map/all_gather | solution.py:126
  20.6 30.0 %copy-start.2 = (bf16[256,512]{1,0:T(8,128)(2,1)S(1)}, bf16[256,512]{1,0:T(8,128)(2,1)}, u32[]{:S(2)}) copy-start(bf16[256,512]{1,0:T(8,128)(2,1)} %param.18) | copy-start | bytes 786436
  20.6 30.2 %copy-start.4 = (f32[512]{0:T(512)S(1)}, f32[512]{0:T(512)}, u32[]{:S(2)}) copy-start(f32[512]{0:T(512)} %param.22) | copy-start | bytes 6148
  20.6 30.2 %copy-start.5 = (f32[256,4]{0,1:T(4,128)S(1)}, f32[256,4]{0,1:T(4,128)}, u32[]{:S(2)}) copy-start(f32[256,4]{0,1:T(4,128)} %param.21) | copy-start | bytes 12292
  50.6 74.1 %all-gather.10.cloned.1.call-start = ((), (), s32[]{:S(2)}) async-start(), calls=%async_computation.6 | async-start | bytes 1179648 | tf_op jit(solution)/shard_map/all_gather | solution.py:14
  53.9 7.6 %copy-start.1 = (bf16[256,512]{1,0:T(8,128)(2,1)S(1)}, bf16[256,512]{1,0:T(8,128)(2,1)}, u32[]{:S(2)}) copy-start(bf16[256,512]{1,0:T(8,128)(2,1)} %param.19) | copy-start | bytes 786436
  62.9 90.8 %reduce-scatter.2.cloned.1.call-start = ((), (), s32[]{:S(2)}) async-start(), calls=%async_computation.5 | async-start | bytes 3276800 | tf_op jit(solution)/shard_map/reduce_scatter | solution.py:131
  94.8 26.5 %copy-start.3 = (bf16[256,512]{1,0:T(8,128)(2,1)S(1)}, bf16[256,512]{1,0:T(8,128)(2,1)}, u32[]{:S(2)}) copy-start(bf16[256,512]{1,0:T(8,128)(2,1)} %param.20) | copy-start | bytes 786436
  94.8 77.6 %all-gather.6.cloned.1.call-start = ((), (), s32[]{:S(2)}) async-start(), calls=%async_computation.3 | async-start | bytes 1310720 | tf_op jit(solution)/shard_map/all_gather | solution.py:88
  124.7 2.9 %copy-start.7 = (f32[128]{0:T(128)S(1)}, f32[128]{0:T(128)}, u32[]{:S(2)}) copy-start(f32[128]{0:T(128)} %param.23) | copy-start | bytes 1540
  125.4 33.8 %copy-start.6 = (f32[256,2]{0,1:T(2,128)S(1)}, f32[256,2]{0,1:T(2,128)}, u32[]{:S(2)}) copy-start(f32[256,2]{0,1:T(2,128)} %param.28) | copy-start | bytes 6148
  153.7 23.6 %all-to-all-start.1 = ((bf16[8,80,512]{2,1,0:T(8,128)(2,1)}), bf16[8,80,512]{2,1,0:T(8,128)(2,1)S(1)}, u32[]{:S(2)}, u32[]{:S(2)}) async-start(bf16[8,80,512]{2,1,0:T(8,128)(2,1)} %bitcast.123), calls=%async_computation.2 | async-start | bytes 1310720 | tf_op jit(solution)/shard_map/all_to_all | solution.py:134
Sparse Core Ops, SparseCore 0:
  50.7 24.2 all-gather.7
  77.7 40.3 all-gather.9
  120.5 33.0 reduce-scatter.1
  155.7 16.6 all-gather.5
